TPU v7x, 512 devices: a whole 4x4x16 slice. The times are simulated.
512 devices in a mesh: ep: 16 (over y, x), tp: 32 (over z, core).
Axes of the slice: x: 4, y: 4, z: 16, core: 2. Of those that a mesh axis runs over, the one named last changes fastest.
Arguments:
- tokens: bfloat16 [2048, 4096], P('ep', 'tp'), may hold values from -16 to 16
- routing: int32 [2048, 4], P('ep'), may hold values from 0 to 31, all different within a row; in each aligned block of 128 rows (0 to 127, 128 to 255, ...) at most 32 rows name the same one
- gate_weights: float32 [2048, 4], P('ep'), may hold values from 0.1 to 1
- w_gate: bfloat16 [32, 1024, 4096], P('ep', 'tp'), may hold values from -0.09375 to 0.09375
- w_up: bfloat16 [32, 1024, 4096], P('ep', 'tp'), may hold values from -0.09375 to 0.09375
- w_down: bfloat16 [32, 1024, 4096], P('ep', None, 'tp'), may hold values from -2 to 2
- out_gain: float32 [4096], P('tp'), may hold values from 0.1 to 1.9
Outputs:
- mixed: bfloat16 [2048, 4096], P('ep', 'tp')
Inputs may be any that keep to these rules, and one draw needn't show every extreme that they name: `routing`: in each aligned block of 128 rows (the tokens of one index of ep) no expert is named by more than 32 entries, and in every draw some expert is named by exactly 32 entries of some block. The 4 entries of a row differ.
All inputs are finite; a program needn't handle non-finite values.
Results may differ from a plain program's by a relative error of at most 0.0057.
Values may be sent and summed in bfloat16 or wider, within the bound.
A program may use at most 64 MiB of HBM per device.

v0:
```python
import jax
import jax.numpy as jnp
from jax import lax
from jax.sharding import PartitionSpec as P

D = 4096
TOPK = 4
EXP_DEV = 2
norm_eps = 1e-05


def from_everyone(value, axis):
    length = lax.axis_size(axis)
    return lax.all_to_all(
        jnp.broadcast_to(value[None], (length, *value.shape)), axis, 0, 0, tiled=True
    )


def taken_together(value, axis):
    return from_everyone(value, axis).sum(axis=0)


def body(tokens, routing, gate_weights, w_gate, w_up, w_down, out_gain):
    ep_count = lax.axis_size("ep")
    tok_rows = tokens.shape[0]
    width_part = tokens.shape[1]
    experts = EXP_DEV * ep_count
    slot_count = 2 * tok_rows * TOPK // experts
    span_rows = ep_count * slot_count
    total_slots = EXP_DEV * span_rows
    flat_route = routing.reshape(-1)
    expert_ids = jnp.arange(experts, dtype=jnp.int32)
    hit_table = (flat_route[:, None] == expert_ids[None, :]).astype(jnp.int32)
    running = jnp.cumsum(hit_table, axis=0) - hit_table
    slot_rank = jnp.sum(running * hit_table, axis=1)
    slot_target = flat_route % EXP_DEV * span_rows + flat_route // EXP_DEV * slot_count + slot_rank
    entry_targets = slot_target.reshape(tok_rows, TOPK)
    slot_ids = jnp.arange(total_slots, dtype=jnp.int32)
    select_table = jnp.any(entry_targets[None, :, :] == slot_ids[:, None, None], axis=2).astype(
        jnp.bfloat16
    )
    outgoing = jnp.dot(select_table, tokens, preferred_element_type=jnp.float32).astype(
        jnp.bfloat16
    )
    outgoing = outgoing.reshape(EXP_DEV, ep_count, slot_count, width_part)
    arrived = lax.all_to_all(outgoing, "ep", split_axis=1, concat_axis=1, tiled=True).reshape(
        EXP_DEV, span_rows, width_part
    )
    piece_cols = lax.all_gather(arrived, "tp", axis=2, tiled=True)
    gate_sum = jnp.einsum("efn,esn->efs", w_gate, piece_cols, preferred_element_type=jnp.float32)
    up_sum = jnp.einsum("efn,esn->efs", w_up, piece_cols, preferred_element_type=jnp.float32)
    square_sum = jnp.einsum(
        "esn,esn->es", piece_cols, piece_cols, preferred_element_type=jnp.float32
    )
    row_scale = lax.rsqrt(square_sum / D + norm_eps)[:, None, :]
    hidden = (jax.nn.silu(gate_sum * row_scale) * (up_sum * row_scale)).astype(jnp.bfloat16)
    out_part = w_down.shape[2]
    expert_out = jnp.einsum(
        "ens,end->esd",
        lax.all_gather(hidden, "tp", axis=1, tiled=True),
        w_down,
        preferred_element_type=jnp.float32,
    ).astype(jnp.bfloat16)
    returned = lax.all_to_all(
        expert_out.reshape(EXP_DEV, ep_count, slot_count, out_part),
        "ep",
        split_axis=1,
        concat_axis=1,
        tiled=True,
    )
    returned = returned.reshape(total_slots, out_part)
    chosen = returned[slot_target].astype(jnp.float32).reshape(tok_rows, TOPK, out_part)
    combined = jnp.sum(chosen * gate_weights[:, :, None], axis=1)
    square_total = taken_together(jnp.sum(combined * combined, axis=1), "tp")
    final_scale = lax.rsqrt(square_total / D + norm_eps)
    return (combined * final_scale[:, None] * out_gain[None, :]).astype(jnp.bfloat16)


def solution(mesh):
    placed = (
        P("ep", "tp"),
        P("ep", None),
        P("ep", None),
        P("ep", "tp", None),
        P("ep", "tp", None),
        P("ep", None, "tp"),
        P("tp"),
    )
    return jax.shard_map(body, mesh=mesh, in_specs=placed, out_specs=P("ep", "tp"), check_vma=False)
```

profile of v0, /device:TPU:1, one launch (start us, length us, event | category | flops | bytes accessed | tf_op | source)
XLA Modules:
  0.0 253.4 jit_solution(5410838036807146994)
XLA Ops:
  6.5 0.9 copy.73
  7.6 1.2 reduce-window.6
  8.8 0.2 slice_reduce_fusion
  9.2 0.1 reduce_sum.41
  9.4 0.7 fusion.13
  10.1 0.4 fusion.1
  10.4 1.0 convolution_convert_fusion.1
  11.5 14.9 %all_to_all.16 = bf16[2,16,32,128]{3,2,0,1:T(8,128)(2,1)S(1)} all-to-all(bf16[2,16,32,128]{3,2,0,1:T(8,128)(2,1)S(1)} %copy.77), channel_id=1, replica_groups=mesh['ep'=16,'tp'=32] {'ep'}, dimensions={1} | all-to-all | bytes 524288 | tf_op jit(solution)/shard_map/all_to_all | solution.py:46
  26.4 0.7 copy.78
  27.2 98.1 %all-gather.3.cloned.1.call-done = bf16[2,512,4096]{2,1,0:T(8,128)(2,1)} async-done(((bf16[2,512,128]{2,1,0:T(8,128)(2,1)}), bf16[2,512,4096]{2,1,0:T(8,128)(2,1)}) %all-gather.3.cloned.1.call-update) | async-done | bytes 8388624 | tf_op jit(solution)/shard_map/all_gather | solution.py:49
  125.2 5.2 %fusion = f32[2,512]{1,0:T(2,128)S(1)} fusion(bf16[2,512,4096]{2,1,0:T(8,128)(2,1)} %all-gather.3.cloned.1.call-done), kind=kLoop, calls=%fused_computation.2 | loop fusion | flops 12581888 | bytes 8392704 | tf_op jit(solution)/shard_map/esn,esn->es/dot_general | solution.py:52
  130.5 0.5 copy-done.1
  131.0 2.6 %fusion.3 = f32[2,32,512]{2,1,0:T(8,128)S(1)} fusion(bf16[2,512,4096]{2,1,0:T(8,128)(2,1)S(1)} %copy-done.1, bf16[2,32,4096]{2,1,0:T(8,128)(2,1)S(1)} %copy-done.2, f32[2,512]{1,0:T(2,128)S(1)} %add_rsqrt_fusion), kind=kOutput, calls=%fused_computation.10 | convolution fusion | flops 268468224 | bytes 9048064 | tf_op jit(solution)/shard_map/efn,esn->efs/dot_general | solution.py:50
  133.7 3.2 %fusion.5 = bf16[2,32,512]{2,1,0:T(8,128)(2,1)} fusion(bf16[2,512,4096]{2,1,0:T(8,128)(2,1)S(1)} %copy-done.1, bf16[2,32,4096]{2,1,0:T(8,128)(2,1)S(1)} %copy-done.3, f32[2,32,512]{2,1,0:T(8,128)S(1)} %fusion.3, f32[2,512]{1,0:T(2,128)S(1)} %add_rsqrt_fusion), kind=kOutput, calls=%fused_computation.12 | convolution fusion | flops 268664832 | bytes 9113600 | tf_op jit(solution)/shard_map/efn,esn->efs/dot_general | solution.py:51
  137.0 0.1 copy.82
  137.2 67.7 %all-gather.5.cloned.1.call-done = bf16[2,1024,512]{2,1,0:T(8,128)(2,1)} async-done(((bf16[2,32,512]{2,1,0:T(8,128)(2,1)}), bf16[2,1024,512]{2,1,0:T(8,128)(2,1)}) %all-gather.5.cloned.1.call-update) | async-done | bytes 2097168 | tf_op jit(solution)/shard_map/all_gather | solution.py:60
  204.9 2.5 convolution_convert_fusion
  207.4 0.7 copy.79
  208.1 6.5 %all-to-all-start.1 = ((bf16[2,16,32,128]{3,2,0,1:T(8,128)(2,1)}), bf16[2,16,32,128]{3,2,0,1:T(8,128)(2,1)S(1)}, u32[]{:S(2)}, u32[]{:S(2)}) async-start(bf16[2,16,32,128]{3,2,0,1:T(8,128)(2,1)} %copy.79), calls=%async_computation.1 | async-start | bytes 524288 | tf_op jit(solution)/shard_map/all_to_all | solution.py:64
  214.7 8.2 %all-to-all-done.1 = bf16[2,16,32,128]{3,2,0,1:T(8,128)(2,1)S(1)} async-done(((bf16[2,16,32,128]{3,2,0,1:T(8,128)(2,1)}), bf16[2,16,32,128]{3,2,0,1:T(8,128)(2,1)S(1)}, u32[]{:S(2)}, u32[]{:S(2)}) %all-to-all-start.1) | async-done | bytes 262176 | tf_op jit(solution)/shard_map/all_to_all | solution.py:64
  222.9 1.3 gather_fusion
  224.2 0.2 fusion.6
  224.6 21.2 %all_to_all.17 = f32[32,1,128]{2,1,0:T(1,128)S(1)} all-to-all(f32[32,1,128]{2,1,0:T(1,128)S(1)} %broadcast_in_dim.2), channel_id=1, replica_groups=mesh['ep'=16,'tp'=32] {'tp'}, dimensions={0} | all-to-all | bytes 32768 | tf_op jit(solution)/shard_map/all_to_all | solution.py:14
  245.9 0.7 multiply_convert_fusion
  (32 shorter events, 0.9 us)
Async XLA Ops:
  6.5 198.4 %copy-start = (bf16[2,1024,128]{2,1,0:T(8,128)(2,1)S(1)}, bf16[2,1024,128]{2,1,0:T(8,128)(2,1)}, u32[]{:S(2)}) copy-start(bf16[2,1024,128]{2,1,0:T(8,128)(2,1)} %param.12) | copy-start | bytes 1572868
  6.5 124.0 %copy-start.2 = (bf16[2,32,4096]{2,1,0:T(8,128)(2,1)S(1)}, bf16[2,32,4096]{2,1,0:T(8,128)(2,1)}, u32[]{:S(2)}) copy-start(bf16[2,32,4096]{2,1,0:T(8,128)(2,1)} %param.10) | copy-start | bytes 1572868
  6.5 118.7 %all-gather.3.cloned.1.call-start = ((), (), s32[]{:S(2)}) async-start(), calls=%async_computation.3 | async-start | bytes 8650752 | tf_op jit(solution)/shard_map/all_gather | solution.py:49
  27.1 177.8 %all-gather.5.cloned.1.call-start = ((), (), s32[]{:S(2)}) async-start(), calls=%async_computation.4 | async-start | bytes 2162688 | tf_op jit(solution)/shard_map/all_gather | solution.py:60
  125.2 5.8 %copy-start.1 = (bf16[2,512,4096]{2,1,0:T(8,128)(2,1)S(1)}, bf16[2,512,4096]{2,1,0:T(8,128)(2,1)}, u32[]{:S(2)}) copy-start(bf16[2,512,4096]{2,1,0:T(8,128)(2,1)} %all-gather.3.cloned.1.call-done) | copy-start | bytes 25165828
  125.2 8.4 %copy-start.3 = (bf16[2,32,4096]{2,1,0:T(8,128)(2,1)S(1)}, bf16[2,32,4096]{2,1,0:T(8,128)(2,1)}, u32[]{:S(2)}) copy-start(bf16[2,32,4096]{2,1,0:T(8,128)(2,1)} %param.11) | copy-start | bytes 1572868
  131.0 6.0 %copy-start.4 = (f32[128,4]{0,1:T(4,128)S(1)}, f32[128,4]{0,1:T(4,128)}, u32[]{:S(2)}) copy-start(f32[128,4]{0,1:T(4,128)} %param.9) | copy-start | bytes 6148
  133.7 112.2 %copy-start.5 = (f32[128]{0:T(128)S(1)}, f32[128]{0:T(128)}, u32[]{:S(2)}) copy-start(f32[128]{0:T(128)} %param.13) | copy-start | bytes 1540
  208.1 14.7 %all-to-all-start.1 = ((bf16[2,16,32,128]{3,2,0,1:T(8,128)(2,1)}), bf16[2,16,32,128]{3,2,0,1:T(8,128)(2,1)S(1)}, u32[]{:S(2)}, u32[]{:S(2)}) async-start(bf16[2,16,32,128]{3,2,0,1:T(8,128)(2,1)} %copy.79), calls=%async_computation.1 | async-start | bytes 524288 | tf_op jit(solution)/shard_map/all_to_all | solution.py:64
Sparse Core Ops, SparseCore 0:
  27.2 97.9 all-gather.2
  137.0 67.7 all-gather.4
where the time goes:
time: 254 us; the launch traced here: 253 us
  waiting for transfers between devices  174 us (69%)
  blocking collectives  36.1 us (14%)
  between operations  13.5 us (5%)
  matrix products  9.35 us (4%)
  other arithmetic  8.73 us (3%)
  starting transfers between devices  6.57 us (3%)
  local copies, waits for them, and re-layouts  5.09 us (2%)
    all_gather x1, waiting for transfers between devices, body(): piece_cols = lax.all_gather(arrived, 'tp', axis=2, tiled=True)  98.1 us
    all_gather x1, waiting for transfers between devices, body(): lax.all_gather(hidden, 'tp', axis=1, tiled=True)  67.7 us
    all_to_all x1, blocking collectives, from_everyone(): lax.all_to_all(jnp.broadcast_to(value[None], (length, *value.shape)), axi...  21.2 us
    all_to_all x1, blocking collectives, body(): lax.all_to_all(outgoing, 'ep', split_axis=1, concat_axis=1, tiled=True)  14.9 us
    all_to_all x1, waiting for transfers between devices, body(): lax.all_to_all(expert_out.reshape(EXP_DEV, ep_count, slot_count, out_part...  8.16 us
    all_to_all x1, starting transfers between devices, body(): lax.all_to_all(expert_out.reshape(EXP_DEV, ep_count, slot_count, out_part...  6.53 us
    dot_general x1, other arithmetic, body(): jnp.einsum('esn,esn->es', piece_cols, piece_cols, preferred_element_type=...  5.23 us
  transfers between devices with their start and end apart: 3, of which 3 were waited for; matrix products, arithmetic and copies ran while one was open for 0% of the time, Pallas kernels for 0%

commit v1 on v0

--- a/solution.py
+++ b/solution.py
@@ -46,7 +46,9 @@
     arrived = lax.all_to_all(outgoing, "ep", split_axis=1, concat_axis=1, tiled=True).reshape(
         EXP_DEV, span_rows, width_part
     )
-    piece_cols = lax.all_gather(arrived, "tp", axis=2, tiled=True)
+    piece_cols = jnp.concatenate(
+        lax.all_to_all(jnp.stack([arrived] * lax.axis_size("tp")), "tp", 0, 0), axis=2
+    )
     gate_sum = jnp.einsum("efn,esn->efs", w_gate, piece_cols, preferred_element_type=jnp.float32)
     up_sum = jnp.einsum("efn,esn->efs", w_up, piece_cols, preferred_element_type=jnp.float32)
     square_sum = jnp.einsum(

time: 254 us -> 532 us (2.09)
  blocking collectives: 36.1 us -> 424 us
  waiting for transfers between devices: 174 us -> 67.8 us
    all_to_all x0 -> x1, blocking collectives: none -> 387 us  [body(): lax.all_to_all(jnp.stack([arrived] * lax.axis_size('tp')), 'tp', 0, 0)]
    all_gather x1 -> x0, waiting for transfers between devices: 98.1 us -> none  [body(): piece_cols = lax.all_gather(arrived, 'tp', axis=2, tiled=True)]
    all_gather x1, waiting for transfers between devices: 67.7 us -> 59.6 us  [body(): lax.all_gather(hidden, 'tp', axis=1, tiled=True)]
  transfers between devices with their start and end apart: 3 -> 2, of which waited for: 3 -> 2; matrix products, arithmetic and copies ran while one was open for 0% -> 0% of each run, Pallas kernels for 0% -> 0%
where the time goes in v1:
time: 532 us
  blocking collectives  424 us (80%)
  waiting for transfers between devices  67.8 us (13%)
  between operations  13.5 us (3%)
  matrix products  9.17 us (2%)
  starting transfers between devices  6.53 us (1%)
  local copies, waits for them, and re-layouts  5.87 us (1%)
    all_to_all x1, blocking collectives, body(): lax.all_to_all(jnp.stack([arrived] * lax.axis_size('tp')), 'tp', 0, 0)  387 us
    all_gather x1, waiting for transfers between devices, body(): lax.all_gather(hidden, 'tp', axis=1, tiled=True)  59.6 us
    all_to_all x1, blocking collectives, from_everyone(): lax.all_to_all(jnp.broadcast_to(value[None], (length, *value.shape)), axi...  21.2 us
    all_to_all x1, blocking collectives, body(): lax.all_to_all(outgoing, 'ep', split_axis=1, concat_axis=1, tiled=True)  14.9 us
  transfers between devices with their start and end apart: 2, of which 2 were waited for; matrix products, arithmetic and copies ran while one was open for 0% of the time, Pallas kernels for 0%

profile of v1, /device:TPU:1, one launch (start us, length us, event | category | flops | bytes accessed | tf_op | source)
XLA Modules:
  0.0 531.7 jit_solution(17995308172807580456)
XLA Ops:
  6.5 0.8 copy.92
  7.6 1.2 reduce-window.6
  8.8 0.2 slice_reduce_fusion
  9.0 0.1 fusion.29
  9.2 0.1 reduce_sum.41
  9.3 0.7 fusion.33
  10.1 0.4 fusion.7
  10.4 1.0 convolution_convert_fusion.1
  11.4 14.9 %all_to_all.21 = bf16[2,16,32,128]{3,2,0,1:T(8,128)(2,1)S(1)} all-to-all(bf16[2,16,32,128]{3,2,0,1:T(8,128)(2,1)S(1)} %copy.96), channel_id=1, replica_groups=mesh['ep'=16,'tp'=32] {'ep'}, dimensions={1} | all-to-all | bytes 524288 | tf_op jit(solution)/shard_map/all_to_all | solution.py:46
  26.4 2.0 stack.3
  28.4 387.4 %all_to_all.22 = bf16[32,2,512,128]{3,2,1,0:T(8,128)(2,1)S(1)} all-to-all(bf16[32,2,512,128]{3,2,1,0:T(8,128)(2,1)S(1)} %stack.3), channel_id=1, replica_groups=mesh['ep'=16,'tp'=32] {'tp'}, dimensions={0} | all-to-all | bytes 16777216 | tf_op jit(solution)/shard_map/all_to_all | solution.py:50
  415.8 1.7 fusion
  417.6 2.5 fusion.11
  420.1 3.2 fusion.23
  423.4 0.1 copy.102
  423.6 59.6 %all-gather.2.cloned.1.call-done = bf16[2,1024,512]{2,1,0:T(8,128)(2,1)} async-done(((bf16[2,32,512]{2,1,0:T(8,128)(2,1)}), bf16[2,1024,512]{2,1,0:T(8,128)(2,1)}) %all-gather.2.cloned.1.call-update) | async-done | bytes 2097168 | tf_op jit(solution)/shard_map/all_gather | solution.py:62
  483.2 2.5 convolution_convert_fusion
  485.7 0.7 copy.99
  486.4 6.5 %all-to-all-start.2 = ((bf16[2,16,32,128]{3,2,0,1:T(8,128)(2,1)}), bf16[2,16,32,128]{3,2,0,1:T(8,128)(2,1)S(1)}, u32[]{:S(2)}, u32[]{:S(2)}) async-start(bf16[2,16,32,128]{3,2,0,1:T(8,128)(2,1)} %copy.99), calls=%async_computation.2 | async-start | bytes 524288 | tf_op jit(solution)/shard_map/all_to_all | solution.py:66
  493.0 8.2 %all-to-all-done.2 = bf16[2,16,32,128]{3,2,0,1:T(8,128)(2,1)S(1)} async-done(((bf16[2,16,32,128]{3,2,0,1:T(8,128)(2,1)}), bf16[2,16,32,128]{3,2,0,1:T(8,128)(2,1)S(1)}, u32[]{:S(2)}, u32[]{:S(2)}) %all-to-all-start.2) | async-done | bytes 262176 | tf_op jit(solution)/shard_map/all_to_all | solution.py:66
  501.2 1.3 gather_fusion
  502.5 0.2 fusion.26
  502.9 21.2 %all_to_all.23 = f32[32,1,128]{2,1,0:T(1,128)S(1)} all-to-all(f32[32,1,128]{2,1,0:T(1,128)S(1)} %broadcast_in_dim.2), channel_id=1, replica_groups=mesh['ep'=16,'tp'=32] {'tp'}, dimensions={0} | all-to-all | bytes 32768 | tf_op jit(solution)/shard_map/all_to_all | solution.py:14
  524.1 0.7 multiply_convert_fusion
  (29 shorter events, 0.7 us)
Async XLA Ops:
  6.5 476.6 %copy-start = (bf16[2,1024,128]{2,1,0:T(8,128)(2,1)S(1)}, bf16[2,1024,128]{2,1,0:T(8,128)(2,1)}, u32[]{:S(2)}) copy-start(bf16[2,1024,128]{2,1,0:T(8,128)(2,1)} %param.12) | copy-start | bytes 1572868
  6.5 476.6 %all-gather.2.cloned.1.call-start = ((), (), s32[]{:S(2)}) async-start(), calls=%async_computation.4 | async-start | bytes 2162688 | tf_op jit(solution)/shard_map/all_gather | solution.py:62
  415.8 1.7 copy-start.3
  415.8 4.3 copy-start.4
  420.1 3.3 copy-start.1
  420.1 104.0 %copy-start.2 = (f32[128]{0:T(128)S(1)}, f32[128]{0:T(128)}, u32[]{:S(2)}) copy-start(f32[128]{0:T(128)} %param.13) | copy-start | bytes 1540
  486.4 14.7 %all-to-all-start.2 = ((bf16[2,16,32,128]{3,2,0,1:T(8,128)(2,1)}), bf16[2,16,32,128]{3,2,0,1:T(8,128)(2,1)S(1)}, u32[]{:S(2)}, u32[]{:S(2)}) async-start(bf16[2,16,32,128]{3,2,0,1:T(8,128)(2,1)} %copy.99), calls=%async_computation.2 | async-start | bytes 524288 | tf_op jit(solution)/shard_map/all_to_all | solution.py:66
Sparse Core Ops, SparseCore 0:
  423.4 59.6 all-gather.1
